TPU v7x, 32 devices: a whole 2x2x4 slice. The times are simulated.
32 devices in a mesh: kv: 4 (over z), tp: 8 (over y, x, core).
Axes of the slice: x: 2, y: 2, z: 4, core: 2. Of those that a mesh axis runs over, the one named last changes fastest.
Arguments:
- piece_tokens: bfloat16 [512, 2048], P('kv'), may hold values from -6 to 6
- dec_tokens: bfloat16 [8, 2048], P('kv'), may hold values from -6 to 6
- norm_gain: float32 [2048], replicated, may hold values from 0.1 to 1.9
- w_query_nope: bfloat16 [2048, 2048], P(None, 'tp'), may hold values from -0.125 to 0.125
- w_query_rope: bfloat16 [2048, 1024], P(None, 'tp'), may hold values from -0.125 to 0.125
- w_latent: bfloat16 [2048, 512], replicated, may hold values from -0.125 to 0.125
- w_key_rope: bfloat16 [2048, 64], replicated, may hold values from -0.125 to 0.125
- latent_gain: float32 [512], replicated, may hold values from 0.1 to 1.9
- w_key_up: bfloat16 [16, 128, 512], P('tp'), may hold values from -0.5 to 0.5
- w_value_up: bfloat16 [16, 512, 128], P('tp'), may hold values from -3 to 3
- w_out: bfloat16 [2048, 2048], P(None, 'tp'), may hold values from -0.25 to 0.25
- prompt_latent: bfloat16 [2048, 512], P('kv'), may hold values from -210 to 210
- prompt_rope: bfloat16 [2048, 64], P('kv'), may hold values from -6 to 6
- dec_latent: bfloat16 [8, 1024, 512], P('kv'), may hold values from -210 to 210
- dec_rope: bfloat16 [8, 1024, 64], P('kv'), may hold values from -6 to 6
- dec_lengths: int32 [8], P('kv'), may hold values from 1 to 1024, 4096 in all
Outputs:
- piece_out: bfloat16 [512, 2048], P('kv', 'tp')
- dec_out: bfloat16 [8, 2048], P('kv', 'tp')
Inputs may be any that keep to these rules, and one draw needn't show every extreme that they name: `dec_lengths`: every decoding sequence has at least one live cache slot, and some sequence has all 1024.
All inputs are finite; a program needn't handle non-finite values. No bound on the sum of `dec_lengths` on one device may be relied on, other than what follows from the above.
Results may differ from a plain program's by a relative error of at most 0.025.
Values may be sent and summed in bfloat16 or wider, within the bound.
A program may use at most 128 MiB of HBM per device.

v0:
```python
import functools

import jax
import jax.numpy as jnp
import numpy as np
from jax import lax
from jax.experimental import pallas as pl
from jax.experimental.pallas import tpu as pltpu
from jax.sharding import PartitionSpec as P

epsilon = 1e-06
rope_base = 10000.0
masked = -1e30
F32 = jnp.float32
BF16 = jnp.bfloat16


def dot(a, b):
    return jnp.dot(a, b, preferred_element_type=F32)


def dot_t(a, b):
    return lax.dot_general(a, b, (((1,), (1,)), ((), ())), preferred_element_type=F32)


def normalize(values, gain_vec):
    mean_sq = jnp.mean(values * values, axis=-1, keepdims=True)
    return values * lax.rsqrt(mean_sq + epsilon) * gain_vec


def kernel(n_kv, n_tp, heads, pad, *refs):
    (
        lengths_hbm, freq_hbm, gain_hbm, lgain_hbm, dec_tok_hbm,
        tok_hbm, wqn_hbm, wqr_hbm, wlat_hbm, wkr_hbm, wku_hbm, wvu_hbm, wout_hbm,
        plat_hbm, prope_hbm, dlat_hbm, drope_hbm,
        out_ref, dec_out_ref,
        lengths, freq_ref, gain_ref, lgain_ref, dec_tok_ref,
        tok, wqn, wqr, wlat, wkr, wku, wvu, wout, klat, prope, dlat, drope,
        normed, krot, qbuf, obuf, ostat, pbuf, sbuf, att,
        load_sem, q_send, q_recv, p_send, p_recv, s_send, s_recv, d_send, d_recv, a_send, a_recv,
    ) = refs
    rows = tok.shape[0]
    cached = plat_hbm.shape[0]
    latent_dim = wlat.shape[1]
    rope = wkr_hbm.shape[0]
    nope = wku.shape[1]
    vdim = wvu.shape[2]
    dec_rows = dec_tok_ref.shape[0]
    dec_keys = dlat.shape[1]
    nope_width = heads * nope
    rot_width = heads * rope
    scale = (nope + rope) ** (-0.5)
    me = lax.axis_index("kv")
    my_t = lax.axis_index("tp")

    loads = {}
    copies = range(heads)
    band = [pl.ds(h * rope, rope) for h in copies]
    sources = (
        ("small", [(freq_hbm, freq_ref), (gain_hbm, gain_ref), (dec_tok_hbm, dec_tok_ref)]),
        ("lengths", [(lengths_hbm, lengths)]), ("tok", [(tok_hbm, tok)]), ("wqn", [(wqn_hbm, wqn)]), ("wqr", [(wqr_hbm, wqr)]),
        ("wlat", [(wlat_hbm, wlat)]), ("lgain", [(lgain_hbm, lgain_ref)]), ("wkr", [(wkr_hbm, wkr.at[band[h]]) for h in copies]),
        ("prope", [(prope_hbm, prope.at[band[h]]) for h in copies]),
        ("plat", [(plat_hbm, klat.at[pl.ds(0, cached)])]), ("wku", [(wku_hbm, wku)]),
        ("wvu", [(wvu_hbm, wvu)]), ("dlat", [(dlat_hbm, dlat)]),
        ("drope", [(drope_hbm, drope.at[:, band[h]]) for h in copies]),
        ("wout", [(wout_hbm, wout)]),
    )
    count = 0
    for name, pairs in sources:
        loads[name] = []
        for src, dst in pairs:
            loads[name].append(pltpu.make_async_copy(src, dst, load_sem.at[count]))
            loads[name][-1].start()
            count += 1

    def loaded(name):
        for copy in loads[name]:
            copy.wait()

    barrier = pltpu.get_barrier_semaphore()
    for d in range(1, n_kv):
        pl.semaphore_signal(
            barrier, inc=1, device_id={"kv": lax.rem(me + d, n_kv)},
            device_id_type=pl.DeviceIdType.MESH,
        )
    for d in range(1, n_tp):
        pl.semaphore_signal(
            barrier, inc=1, device_id={"tp": lax.rem(my_t + d, n_tp)},
            device_id_type=pl.DeviceIdType.MESH,
        )

    def remote(src, dst, send, recv, axis, target):
        return pltpu.make_async_remote_copy(
            src_ref=src, dst_ref=dst, send_sem=send, recv_sem=recv,
            device_id={axis: target}, device_id_type=pl.DeviceIdType.MESH,
        )

    loaded("small")
    loaded("lengths")
    row = lax.broadcasted_iota(jnp.int32, (rows + pad, rot_width), 0)
    position = n_kv * cached + me * rows + row
    for b in range(dec_rows):
        position = jnp.where(row == rows + b, lengths[b], position)
    angles = position.astype(F32) * freq_ref[...]
    lane = lax.broadcasted_iota(jnp.int32, (rows + pad, rot_width), 1)
    front = lane % rope < rope // 2
    cosines = jnp.cos(angles)
    sines = jnp.sin(angles)
    sines = jnp.where(front, -sines, sines)

    gain = gain_ref[...]
    normed[pl.ds(rows, pad), :] = jnp.zeros((pad, normed.shape[1]), BF16)
    dec_norm = normalize(dec_tok_ref[...].astype(F32), gain).astype(BF16)
    normed[pl.ds(rows, dec_rows), :] = dec_norm
    loaded("tok")
    normed[pl.ds(0, rows), :] = normalize(tok[...].astype(F32), gain).astype(BF16)

    def rotated(v):
        half = rope // 2
        swapped = jnp.where(
            front, pltpu.roll(v, rot_width - half, 1), pltpu.roll(v, half, 1)
        )
        return (v * cosines + swapped * sines).astype(BF16)

    x = normed[...]
    loaded("wqn")
    q_nope = dot(x, wqn[...]).astype(BF16)
    loaded("wqr")
    q_rot = rotated(dot(x, wqr[...]))
    qbuf[me, :, 0:nope_width] = q_nope[:rows]
    qbuf[me, :, nope_width:] = q_rot[:rows]

    pl.semaphore_wait(barrier, n_kv + n_tp - 2)

    chunks = q_send.shape[1]
    chunk = rows // chunks
    line = n_kv == 4

    def q_copy(block, target, slot, c):
        part = qbuf.at[block, pl.ds(c * chunk, chunk)]
        return remote(part, part, q_send.at[slot, c], q_recv.at[block, c], "kv", target)

    def q_arrived(block):
        for c in range(chunks):
            q_copy(block, lax.rem(me + 1, n_kv), 0, c).wait_recv()

    upper = me // 2
    middle = lax.rem(me + upper, 2) == 1
    own_end, far_end = 3 * upper, 3 - 3 * upper
    own_middle, far_middle = 1 + upper, 2 - upper
    if line:
        first = jnp.where(middle, far_middle, own_middle)
        second = jnp.where(middle, own_end, far_middle)
        first_served = jnp.where(middle, far_middle, own_middle)
        second_served = jnp.where(middle, far_end, far_middle)
        last_served = jnp.where(middle, own_end, far_end)
        targets = [first, second]
    else:
        targets = [lax.rem(me + d, n_kv) for d in range(1, n_kv)]
    for i, target in enumerate(targets):
        for c in range(chunks):
            q_copy(me, target, i, c).start()

    def hand_on(block, slot):
        if line:
            @pl.when(middle)
            def _():
                for c in range(chunks):
                    q_copy(block, lax.rem(me + 1, n_kv), 0, c).wait_recv()
                    q_copy(block, own_end, slot, c).start()

    loaded("wlat")
    loaded("lgain")
    latent = normalize(dot(x, wlat[...]), lgain_ref[...]).astype(BF16)
    loaded("plat")
    klat[pl.ds(cached, rows), :] = latent[:rows]
    loaded("wkr")
    k_rot = rotated(dot_t(x, wkr[...]))
    krot[...] = k_rot[:rows]
    loaded("prope")
    loaded("wku")
    loaded("wvu")

    def stacked(nope_part, rot_part):
        count = nope_part.shape[0]
        lanes = lax.broadcasted_iota(jnp.int32, (count, rot_width), 1) // rope
        lat = [dot(nope_part[:, h * nope:(h + 1) * nope], wku[h]).astype(BF16) for h in range(heads)]
        rot = [jnp.where(lanes == h, rot_part, jnp.zeros_like(rot_part)) for h in range(heads)]
        return jnp.concatenate(lat, axis=0), jnp.concatenate(rot, axis=0)

    total = heads * rows
    stat_lane = lax.broadcasted_iota(jnp.int32, (total, 128), 1)
    query_row = lax.broadcasted_iota(jnp.int32, (total, rows), 0) % rows
    key_col = lax.broadcasted_iota(jnp.int32, (total, rows), 1)

    def attend(block, j):
        lat, rot = stacked(block[:, :nope_width], block[:, nope_width:])
        s_c = (dot_t(lat, klat[pl.ds(0, cached), :]) + dot(rot, prope[...])) * scale
        s_p = (
            dot_t(lat, klat[pl.ds(cached, rows), :]) + dot_t(rot, krot[...])
        ) * scale
        s_p = jnp.where(me * rows + key_col <= j * rows + query_row, s_p, masked)
        peak = jnp.maximum(
            jnp.max(s_c, axis=1, keepdims=True), jnp.max(s_p, axis=1, keepdims=True)
        )
        w_c = jnp.exp(s_c - peak)
        w_p = jnp.exp(s_p - peak)
        weight_sum = jnp.sum(w_c, axis=1, keepdims=True) + jnp.sum(w_p, axis=1, keepdims=True)
        mixed = (
            dot(w_c.astype(BF16), klat[pl.ds(0, cached), :])
            + dot(w_p.astype(BF16), klat[pl.ds(cached, rows), :])
        ).astype(BF16)
        values = [
            dot(mixed[h * rows:(h + 1) * rows], wvu[h]).astype(BF16) for h in range(heads)
        ]
        stat = jnp.where(stat_lane == 0, peak, jnp.where(stat_lane == 1, weight_sum, 0.0))
        return values, jnp.transpose(stat)[0:2]

    def store(values, stat, value_ref, stat_ref, slot):
        for h in range(heads):
            value_ref[slot, h] = values[h]
        stat_ref[slot] = stat

    values, stat = attend(qbuf[me], me)
    store(values, stat, pbuf, sbuf, me)

    loaded("dlat")
    loaded("drope")
    d_lat, d_rot = stacked(q_nope[rows:], q_rot[rows:])
    own_lat = jnp.concatenate([latent[rows:]] * heads, axis=0).astype(F32)
    own_rot = jnp.concatenate([k_rot[rows:]] * heads, axis=0).astype(F32)
    own_s = (
        jnp.sum(d_lat.astype(F32) * own_lat, axis=1, keepdims=True)
        + jnp.sum(d_rot.astype(F32) * own_rot, axis=1, keepdims=True)
    ) * scale
    row_of = lax.broadcasted_iota(jnp.int32, (heads * pad, 1), 0) % pad
    key_at = lax.broadcasted_iota(jnp.int32, (heads * pad, dec_keys), 1)
    mix = jnp.zeros((heads * pad, latent_dim), F32)
    d_sum = jnp.ones((heads * pad, 1), F32)
    for b in range(dec_rows):
        keys = dlat[b]
        s = (dot_t(d_lat, keys) + dot(d_rot, drope[b])) * scale
        s = jnp.where(key_at < lengths[b], s, masked)
        peak = jnp.maximum(jnp.max(s, axis=1, keepdims=True), own_s)
        w = jnp.exp(s - peak)
        own_w = jnp.exp(own_s - peak)
        mix_b = dot(w.astype(BF16), keys) + own_w.astype(BF16).astype(F32) * own_lat
        sum_b = jnp.sum(w, axis=1, keepdims=True) + own_w
        if b < 2:
            hand_on((far_middle, far_end)[b], 2 + b)
        mix = jnp.where(row_of == b, mix_b, mix)
        d_sum = jnp.where(row_of == b, sum_b, d_sum)
    for b in range(dec_rows, 2):
        hand_on((far_middle, far_end)[b], 2 + b)
    mix = mix.astype(BF16)
    for h in range(heads):
        part = slice(h * pad, (h + 1) * pad)
        d_value = dot(mix[part], wvu[h]).astype(BF16).astype(F32)
        att[my_t, pl.ds(rows, pad), h * vdim:(h + 1) * vdim] = (d_value / d_sum[part]).astype(BF16)

    if n_tp == 8:
        tp_order = [6, 7, 2, 4, 3, 5, 1]
    else:
        tp_order = list(range(1, n_tp))

    def tp_peer(d):
        if n_tp != 8:
            return lax.rem(my_t + d, n_tp)
        high, mid, low = my_t // 4, my_t // 2, my_t
        return (
            lax.rem(high + d // 4, 2) * 4 + lax.rem(mid + d // 2 % 2, 2) * 2 + lax.rem(low + d % 2, 2)
        )

    def dec_part(t):
        return att.at[t, pl.ds(rows, pad), :]

    def head_part(t, h):
        return att.at[t, pl.ds(0, rows), pl.ds(h * vdim, vdim)]

    def dec_copy(d):
        part = dec_part(my_t)
        return remote(part, part, d_send.at[d], d_recv.at[my_t], "tp", tp_peer(d))

    def head_copy(d, h):
        part = head_part(my_t, h)
        return remote(part, part, a_send.at[d, h], a_recv.at[my_t, h], "tp", tp_peer(d))

    for d in tp_order:
        dec_copy(d).start()

    def p_copies(j):
        return [remote(ostat.at[j], sbuf.at[me], s_send.at[j], s_recv.at[me], "kv", j)] + [
            remote(obuf.at[j, h], pbuf.at[me, h], p_send.at[j, h], p_recv.at[me, h], "kv", j)
            for h in range(heads)
        ]

    def serve(j):
        values, stat = attend(qbuf[j], j)
        store(values, stat, obuf, ostat, j)
        for copy in p_copies(j):
            copy.start()

    def serve_at(d):
        j = lax.rem(me + d, n_kv)
        q_arrived(j)
        serve(j)

    if line:
        pl.when(jnp.logical_not(middle))(lambda: q_arrived(own_middle))
        serve(first_served)
        pl.when(jnp.logical_not(middle))(lambda: q_arrived(far_middle))
        serve(second_served)
        q_arrived(last_served)
        serve(last_served)
    else:
        lax.fori_loop(1, n_kv, lambda d, c: (serve_at(d), c)[1], 0)

    for d in range(1, n_kv):
        j = lax.rem(me + d, n_kv)
        remote(ostat.at[j], sbuf.at[j], s_send.at[j], s_recv.at[j], "kv", j).wait_recv()

    peak = sbuf[0, 0:1, :]
    for j in range(1, n_kv):
        peak = jnp.maximum(peak, sbuf[j, 0:1, :])
    factors = [jnp.exp(sbuf[j, 0:1, :] - peak) for j in range(n_kv)]
    whole = factors[0] * sbuf[0, 1:2, :]
    for j in range(1, n_kv):
        whole = whole + factors[j] * sbuf[j, 1:2, :]
    table_row = lax.broadcasted_iota(jnp.int32, (128, total), 0)
    table = jnp.zeros((128, total), F32)
    for j in range(n_kv):
        table = jnp.where(table_row == j, factors[j] / whole, table)
    table = jnp.transpose(table)
    for h in range(heads):
        for d in range(1, n_kv):
            j = lax.rem(me + d, n_kv)
            remote(
                obuf.at[j, h], pbuf.at[j, h], p_send.at[j, h], p_recv.at[j, h], "kv", j
            ).wait_recv()
        acc = jnp.zeros((rows, vdim), F32)
        for j in range(n_kv):
            column = table[h * rows:(h + 1) * rows, j:j + 1]
            acc = acc + column * pbuf[j, h].astype(F32)
        att[my_t, pl.ds(0, rows), h * vdim:(h + 1) * vdim] = acc.astype(BF16)
        for d in tp_order:
            head_copy(d, h).start()

    loaded("wout")
    width = heads * vdim

    def project_out(t):
        return dot(att[t], wout[pl.ds(pl.multiple_of(t * width, width), width), :])

    result = project_out(my_t)
    for d in reversed(tp_order):
        t = tp_peer(d)
        part = dec_part(t)
        remote(part, part, d_send.at[d], d_recv.at[t], "tp", t).wait_recv()
        for h in range(heads):
            part = head_part(t, h)
            remote(part, part, a_send.at[d, h], a_recv.at[t, h], "tp", t).wait_recv()
        result = result + project_out(t)
    result = result.astype(BF16)
    out_ref[...] = result[:rows]
    dec_out_ref[...] = result[rows:rows + dec_rows]

    for i, target in enumerate(targets):
        for c in range(chunks):
            q_copy(me, target, i, c).wait_send()
    if line:
        @pl.when(middle)
        def _():
            for c in range(chunks):
                q_copy(far_middle, own_end, 2, c).wait_send()
                q_copy(far_end, own_end, 3, c).wait_send()
    for d in range(1, n_kv):
        for copy in p_copies(lax.rem(me + d, n_kv)):
            copy.wait_send()
    for d in range(1, n_tp):
        dec_copy(d).wait_send()
        for h in range(heads):
            head_copy(d, h).wait_send()


def shards(
    n_kv, n_tp,
    piece_tokens, dec_tokens, norm_gain, w_query_nope, w_query_rope, w_latent, w_key_rope,
    latent_gain, w_key_up, w_value_up, w_out, prompt_latent, prompt_rope, dec_latent, dec_rope,
    dec_lengths,
):
    rows, width = piece_tokens.shape
    dec_rows = dec_tokens.shape[0]
    pad = -(-dec_rows // 16) * 16
    cached, latent_dim = prompt_latent.shape
    heads, nope, _ = w_key_up.shape
    vdim = w_value_up.shape[2]
    rope = w_key_rope.shape[1]
    half = rope // 2
    frequency = rope_base ** (-np.arange(half) / half)
    frequency = jnp.asarray(np.tile(frequency, 2 * heads)[None, :].astype(np.float32))
    vmem = pl.BlockSpec(memory_space=pltpu.VMEM)
    anywhere = pl.BlockSpec(memory_space=pltpu.HBM)
    sem = pltpu.SemaphoreType.DMA
    scratch = [
        pltpu.SMEM(dec_lengths.shape, jnp.int32),
        pltpu.VMEM(frequency.shape, F32),
        pltpu.VMEM((1, width), F32),
        pltpu.VMEM((1, latent_dim), F32),
        pltpu.VMEM(dec_tokens.shape, BF16),
        pltpu.VMEM(piece_tokens.shape, BF16),
        pltpu.VMEM(w_query_nope.shape, BF16),
        pltpu.VMEM(w_query_rope.shape, BF16),
        pltpu.VMEM(w_latent.shape, BF16),
        pltpu.VMEM((heads * rope, width), BF16),
        pltpu.VMEM(w_key_up.shape, BF16),
        pltpu.VMEM(w_value_up.shape, BF16),
        pltpu.VMEM(w_out.shape, BF16),
        pltpu.VMEM((cached + rows, latent_dim), BF16),
        pltpu.VMEM((heads * rope, cached), BF16),
        pltpu.VMEM(dec_latent.shape, BF16),
        pltpu.VMEM((dec_rows, heads * rope, dec_latent.shape[1]), BF16),
        pltpu.VMEM((rows + pad, width), BF16),
        pltpu.VMEM((rows, heads * rope), BF16),
        pltpu.VMEM((n_kv, rows, heads * (nope + rope)), BF16),
        pltpu.VMEM((n_kv, heads, rows, vdim), BF16),
        pltpu.VMEM((n_kv, 2, heads * rows), F32),
        pltpu.VMEM((n_kv, heads, rows, vdim), BF16),
        pltpu.VMEM((n_kv, 2, heads * rows), F32),
        pltpu.VMEM((n_tp, rows + pad, heads * vdim), BF16),
        sem((14 + 3 * heads,)),
    ] + (
        [sem((n_kv, 4))] * 2 + [sem((n_kv, heads))] * 2 + [sem((n_kv,))] * 2
        + [sem((n_tp,))] * 2 + [sem((n_tp, heads))] * 2
    )
    return pl.pallas_call(
        functools.partial(kernel, n_kv, n_tp, heads, pad),
        out_shape=(
            pltpu.VMEM((rows, w_out.shape[1]), BF16),
            pltpu.VMEM((dec_rows, w_out.shape[1]), BF16),
        ),
        in_specs=[anywhere] * 17,
        out_specs=(vmem, vmem),
        scratch_shapes=scratch,
        compiler_params=pltpu.CompilerParams(
            collective_id=0, has_side_effects=True, vmem_limit_bytes=60 * 1024 * 1024
        ),
    )(
        dec_lengths, frequency, norm_gain[None, :], latent_gain[None, :], dec_tokens,
        piece_tokens, w_query_nope, w_query_rope, w_latent, w_key_rope.T, w_key_up, w_value_up,
        w_out, prompt_latent, prompt_rope.T, dec_latent, jnp.swapaxes(dec_rope, 1, 2),
    )


def solution(mesh):
    in_specs = (
        P("kv", None),
        P("kv", None),
        P(),
        P(None, "tp"),
        P(None, "tp"),
        P(),
        P(),
        P(),
        P("tp", None, None),
        P("tp", None, None),
        P(None, "tp"),
        P("kv", None),
        P("kv", None),
        P("kv", None, None),
        P("kv", None, None),
        P("kv"),
    )
    out_specs = (P("kv", "tp"), P("kv", "tp"))
    body = functools.partial(shards, mesh.shape["kv"], mesh.shape["tp"])
    return jax.shard_map(body, mesh=mesh, in_specs=in_specs, out_specs=out_specs, check_vma=False)
```

profile of v0, /device:TPU:0, one launch (start us, length us, event | category | flops | bytes accessed | tf_op | source)
XLA Modules:
  0.0 29.7 jit_solution(12499453810823842103)
XLA Ops:
  0.6 27.8 %shard_map.176 = (bf16[128,256]{1,0:T(8,128)(2,1)S(1)}, bf16[2,256]{1,0:T(2,128)(2,1)S(1)}) custom-call(s32[2]{0:T(128)} %refs_0_.1, f32[1,128]{1,0:T(1,128)} %constant.2.clone.refs_1_, f32[1,2048]{1,0:T(1,128)} %bitcast.8, f32[1,512]{1,0:T(1,128)} %bitcast.9, bf16[2,2048]{1,0:T(2,128)(2,1)} %refs_4_.1, bf16[128,2048]{1,0:T(8,128)(2,1)} %refs_5_.1, ...), custom_call_target="tpu_custom_call" | custom-call | tf_op jit(solution)/shard_map/pallas_call | solution.py:436
  28.5 0.6 %copy.21 = bf16[128,256]{1,0:T(8,128)(2,1)} copy(bf16[128,256]{1,0:T(8,128)(2,1)S(1)} %get-tuple-element.2) | data formatting | bytes 131072
  29.1 0.6 %copy.22 = bf16[2,256]{1,0:T(2,128)(2,1)} copy(bf16[2,256]{1,0:T(2,128)(2,1)S(1)} %get-tuple-element.3) | data formatting | bytes 2048
where the time goes:
time: 29.8 us; the launch traced here: 29.7 us
  Pallas kernels  27.8 us (93%)
  local copies, waits for them, and re-layouts  1.19 us (4%)
  between operations  0.65 us (2%)
    pallas_call x1, Pallas kernels, shards(): pl.pallas_call(functools.partial(kernel, n_kv, n_tp, heads, pad), out_sha...  27.8 us
    unnamed x2, local copies, waits for them, and re-layouts  1.19 us

commit v1 on v0

--- a/solution.py
+++ b/solution.py
@@ -38,6 +38,7 @@
         tok, wqn, wqr, wlat, wkr, wku, wvu, wout, klat, prope, dlat, drope,
         normed, krot, qbuf, obuf, ostat, pbuf, sbuf, att,
         load_sem, q_send, q_recv, p_send, p_recv, s_send, s_recv, d_send, d_recv, a_send, a_recv,
+        f_send,
     ) = refs
     rows = tok.shape[0]
     cached = plat_hbm.shape[0]
@@ -259,10 +260,15 @@
         d_value = dot(mix[part], wvu[h]).astype(BF16).astype(F32)
         att[my_t, pl.ds(rows, pad), h * vdim:(h + 1) * vdim] = (d_value / d_sum[part]).astype(BF16)
 
-    if n_tp == 8:
+    paired = n_tp == 8
+    if paired:
         tp_order = [6, 7, 2, 4, 3, 5, 1]
+        head_order = [6, 2, 4, 1]
+        relayed = [2, 4, 6]
     else:
         tp_order = list(range(1, n_tp))
+        head_order = tp_order
+        relayed = []
 
     def tp_peer(d):
         if n_tp != 8:
@@ -285,6 +291,10 @@
     def head_copy(d, h):
         part = head_part(my_t, h)
         return remote(part, part, a_send.at[d, h], a_recv.at[my_t, h], "tp", tp_peer(d))
+
+    def relay_copy(d, h):
+        part = head_part(tp_peer(d), h)
+        return remote(part, part, f_send.at[d, h], a_recv.at[tp_peer(d), h], "tp", tp_peer(1))
 
     for d in tp_order:
         dec_copy(d).start()
@@ -343,7 +353,7 @@
             column = table[h * rows:(h + 1) * rows, j:j + 1]
             acc = acc + column * pbuf[j, h].astype(F32)
         att[my_t, pl.ds(0, rows), h * vdim:(h + 1) * vdim] = acc.astype(BF16)
-        for d in tp_order:
+        for d in head_order:
             head_copy(d, h).start()
 
     loaded("wout")
@@ -352,14 +362,22 @@
     def project_out(t):
         return dot(att[t], wout[pl.ds(pl.multiple_of(t * width, width), width), :])
 
+    def head_arrived(d, h):
+        part = head_part(tp_peer(d), h)
+        remote(part, part, a_send.at[d, h], a_recv.at[tp_peer(d), h], "tp", tp_peer(d)).wait_recv()
+
     result = project_out(my_t)
-    for d in reversed(tp_order):
+    for h in range(heads):
+        for d in relayed:
+            head_arrived(d, h)
+            relay_copy(d, h).start()
+    for d in (relayed + [1, 3, 5, 7] if paired else reversed(tp_order)):
         t = tp_peer(d)
         part = dec_part(t)
         remote(part, part, d_send.at[d], d_recv.at[t], "tp", t).wait_recv()
-        for h in range(heads):
-            part = head_part(t, h)
-            remote(part, part, a_send.at[d, h], a_recv.at[t, h], "tp", t).wait_recv()
+        if d not in relayed:
+            for h in range(heads):
+                head_arrived(d, h)
         result = result + project_out(t)
     result = result.astype(BF16)
     out_ref[...] = result[:rows]
@@ -380,7 +398,21 @@
     for d in range(1, n_tp):
         dec_copy(d).wait_send()
         for h in range(heads):
-            head_copy(d, h).wait_send()
+            if d in head_order:
+                head_copy(d, h).wait_send()
+            if d in relayed:
+                relay_copy(d, h).wait_send()
+
+
+def deliver(piece, dec, piece_out, dec_out, sem):
+    copies = [
+        pltpu.make_async_copy(piece, piece_out, sem.at[0]),
+        pltpu.make_async_copy(dec, dec_out, sem.at[1]),
+    ]
+    for copy in copies:
+        copy.start()
+    for copy in copies:
+        copy.wait()
 
 
 def shards(
@@ -431,9 +463,9 @@
         sem((14 + 3 * heads,)),
     ] + (
         [sem((n_kv, 4))] * 2 + [sem((n_kv, heads))] * 2 + [sem((n_kv,))] * 2
-        + [sem((n_tp,))] * 2 + [sem((n_tp, heads))] * 2
+        + [sem((n_tp,))] * 2 + [sem((n_tp, heads))] * 3
     )
-    return pl.pallas_call(
+    results = pl.pallas_call(
         functools.partial(kernel, n_kv, n_tp, heads, pad),
         out_shape=(
             pltpu.VMEM((rows, w_out.shape[1]), BF16),
@@ -450,6 +482,13 @@
         piece_tokens, w_query_nope, w_query_rope, w_latent, w_key_rope.T, w_key_up, w_value_up,
         w_out, prompt_latent, prompt_rope.T, dec_latent, jnp.swapaxes(dec_rope, 1, 2),
     )
+    return pl.pallas_call(
+        deliver,
+        out_shape=tuple(pltpu.HBM(r.shape, r.dtype) for r in results),
+        in_specs=[vmem, vmem],
+        out_specs=(anywhere, anywhere),
+        scratch_shapes=[sem((2,))],
+    )(*[pltpu.with_memory_space_constraint(r, pltpu.VMEM) for r in results])
 
 
 def solution(mesh):

time: 29.8 us -> 28.7 us (0.963)
  local copies, waits for them, and re-layouts: 1.19 us -> 0 us
    unnamed x2 -> x0, local copies, waits for them, and re-layouts: 1.19 us -> none
    pallas_call x0 -> x1, Pallas kernels: none -> 0.65 us  [shards(): pl.pallas_call(deliver, out_shape=tuple((pltpu.HBM(r.shape, r.dtype) for...]
    pallas_call x1, Pallas kernels: 27.8 us -> 27.2 us  [shards(): pl.pallas_call(functools.partial(kernel, n_kv, n_tp, heads, pad), out_sha...]
where the time goes in v1:
time: 28.7 us; the launch traced here: 28.5 us
  Pallas kernels  27.8 us (97%)
  between operations  0.64 us (2%)
    pallas_call x1, Pallas kernels, shards(): pl.pallas_call(functools.partial(kernel, n_kv, n_tp, heads, pad), out_sha...  27.2 us
    pallas_call x1, Pallas kernels, shards(): pl.pallas_call(deliver, out_shape=tuple((pltpu.HBM(r.shape, r.dtype) for...  0.65 us

profile of v1, /device:TPU:0, one launch (start us, length us, event | category | flops | bytes accessed | tf_op | source)
XLA Modules:
  0.0 28.5 jit_solution(3508073537242119852)
XLA Ops:
  0.6 27.2 %shard_map.176 = (bf16[128,256]{1,0:T(8,128)(2,1)S(1)}, bf16[2,256]{1,0:T(2,128)(2,1)S(1)}) custom-call(s32[2]{0:T(128)} %refs_0_.1, f32[1,128]{1,0:T(1,128)} %constant.2.clone.refs_1_, f32[1,2048]{1,0:T(1,128)} %bitcast.8, f32[1,512]{1,0:T(1,128)} %bitcast.9, bf16[2,2048]{1,0:T(2,128)(2,1)} %refs_4_.1, bf16[128,2048]{1,0:T(8,128)(2,1)} %refs_5_.1, ...), custom_call_target="tpu_custom_call" | custom-call | tf_op jit(solution)/shard_map/pallas_call | solution.py:468
  27.8 0.7 %shard_map.177 = (bf16[128,256]{1,0:T(8,128)(2,1)}, bf16[2,256]{1,0:T(2,128)(2,1)}) custom-call(bf16[128,256]{1,0:T(8,128)(2,1)S(1)} %get-tuple-element.4.piece, bf16[2,256]{1,0:T(2,128)(2,1)S(1)} %get-tuple-element.5.dec), custom_call_target="tpu_custom_call" | custom-call | tf_op jit(solution)/shard_map/pallas_call | solution.py:485
